TPU v7x, 32 devices: a whole 2x2x4 slice. The times are simulated.
32 devices in a mesh: fs: 8 (over z, core), tp: 4 (over y, x).
Axes of the slice: x: 2, y: 2, z: 4, core: 2. Of those that a mesh axis runs over, the one named last changes fastest.
Arguments:
- prompt: bfloat16 [1024, 2048], P('tp'), may hold values from -6 to 6
- norm_gain: float32 [2048], P('fs'), may hold values from 0.1 to 1.9
- gate_master: float32 [32, 2048, 512], P(None, 'fs', 'tp'), may hold values from -6 to 6
- up_master: float32 [32, 2048, 512], P(None, 'fs', 'tp'), may hold values from -6 to 6
- down_master: float32 [32, 2048, 512], P(None, 'fs', 'tp'), may hold values from -6 to 6
- group_choice: int32 [1024], P('tp'), may hold values from 0 to 3
- inner_choice: int32 [1024, 2], P('tp'), may hold values from 0 to 7, as said below
- route_weight: float32 [1024, 2], P('tp'), may hold values from 0.2 to 1
Outputs:
- gate_served: bfloat16 [2048, 16384], P(None, 'fs')
- up_served: bfloat16 [2048, 16384], P(None, 'fs')
- down_served: bfloat16 [2048, 16384], P(None, 'fs')
- mixed: bfloat16 [1024, 2048], P('tp', 'fs')
Inputs may be any that keep to these rules, and one draw needn't show every extreme that they name: `inner_choice`: the two experts of a token differ.
All inputs are finite; a program needn't handle non-finite values.
Results may differ from a plain program's by a relative error of at most 0.0081.
Values may be sent and summed in bfloat16 or wider, within the bound.
A program may use at most 128 MiB of HBM per device.

v0:
```python
import jax
import jax.numpy as jnp
from jax import lax
from jax.sharding import PartitionSpec as P

FF = 512
GROUPS = 4
EPG = 8


def flatten_rows(piece):
    count, experts, rows, hidden = piece.shape
    return piece.transpose(0, 2, 1, 3).reshape(count, rows, experts * hidden)


def restore_rows(gathered, rows):
    parts = lax.axis_size("tp")
    count, total, width = gathered.shape
    blocks = total // (parts * rows)
    ordered = gathered.reshape(count, parts, blocks, rows, width).transpose(0, 2, 1, 3, 4)
    return ordered.reshape(count, total, width)


def activations(normed, gate_local, up_local, column_weight):
    width = normed.shape[1]
    gate_act = jnp.dot(normed, gate_local, preferred_element_type=jnp.float32) * width ** (-0.5)
    up_act = jnp.dot(normed, up_local, preferred_element_type=jnp.float32) * width ** (-0.5)
    return (column_weight * jax.nn.silu(gate_act) * up_act).astype(jnp.bfloat16)


def route_columns(weight, columns, experts):
    first = lax.axis_index("fs") * columns
    owner = (first + jnp.arange(columns, dtype=jnp.int32)) // FF
    onehot = (owner[None, :] == jnp.arange(experts, dtype=jnp.int32)[:, None]).astype(jnp.float32)
    return jnp.dot(weight, onehot, precision=lax.Precision.HIGHEST)


def shards(
    prompt, norm_gain, gate_master, up_master, down_master, group_choice, inner_choice, route_weight
):
    experts = GROUPS * EPG
    scale = norm_gain[None, :, None]
    gate_cast = (gate_master * scale).astype(jnp.bfloat16)
    up_cast = (up_master * scale).astype(jnp.bfloat16)
    down_cast = down_master.astype(jnp.bfloat16)
    rows = gate_master.shape[1] // lax.axis_size("tp")
    values = prompt.astype(jnp.float32)
    normed = (values * lax.rsqrt(jnp.mean(values * values, axis=1, keepdims=True) + 1e-06)).astype(
        jnp.bfloat16
    )
    chosen = group_choice[:, None] * EPG + inner_choice
    member = (chosen[:, :, None] == jnp.arange(experts, dtype=jnp.int32)[None, None, :]).astype(
        jnp.float32
    )
    weight = jnp.sum(member * route_weight[:, :, None], axis=1)
    stacked = jnp.stack([gate_cast, up_cast, down_cast])
    widened = lax.all_to_all(stacked, "tp", split_axis=2, concat_axis=3, tiled=True)
    moved = lax.all_to_all(flatten_rows(widened), "fs", split_axis=2, concat_axis=1, tiled=True)
    served = restore_rows(lax.all_gather(moved, "tp", axis=1, tiled=True), rows)
    gate_local, up_local, down_local = (served[0], served[1], served[2])
    column_weight = route_columns(weight, gate_local.shape[1], experts)
    scaled = activations(normed, gate_local, up_local, column_weight)
    summed = lax.psum_scatter(
        lax.dot_general(
            down_local, scaled, (((1,), (1,)), ((), ())), preferred_element_type=jnp.float32
        ),
        "fs",
        scatter_dimension=0,
        tiled=True,
    )
    mixed = (summed * FF ** (-0.5)).T.astype(jnp.bfloat16)
    return (gate_local, up_local, down_local, mixed)


def solution(mesh):
    in_specs = (
        P("tp", None),
        P("fs"),
        P(None, "fs", "tp"),
        P(None, "fs", "tp"),
        P(None, "fs", "tp"),
        P("tp"),
        P("tp", None),
        P("tp", None),
    )
    out_specs = (P(None, "fs"), P(None, "fs"), P(None, "fs"), P("tp", "fs"))
    return jax.shard_map(shards, mesh=mesh, in_specs=in_specs, out_specs=out_specs, check_vma=False)
```

profile of v0, /device:TPU:0, one launch (start us, length us, event | category | flops | bytes accessed | tf_op | source)
XLA Modules:
  0.0 666.3 jit_solution(537520447581431105)
XLA Ops:
  7.2 0.0 copy-start.4
  7.2 0.0 all-gather.2.cloned.1.call-start
  7.2 0.0 copy-start
  7.2 4.8 copy.90
  12.0 0.0 copy-done.4
  12.0 0.0 copy-done
  12.0 9.9 %fusion.6 = (bf16[1,32,256,128]{3,1,0,2:T(8,128)(2,1)S(1)}, bf16[1,32,256,128]{3,1,0,2:T(8,128)(2,1)S(1)}) fusion(f32[32,256,128]{2,1,0:T(8,128)S(1)} %copy-done, f32[256]{0:T(256)S(1)} %copy-done.4, f32[32,256,128]{2,1,0:T(8,128)} %param.11), kind=kLoop, calls=%fused_computation.16 | loop fusion | flops 4194304 | bytes 12583936 | tf_op jit(solution)/shard_map/stack | solution.py:56
  22.0 0.8 pad_maximum_fusion
  22.7 75.3 %all_to_all.36 = bf16[3,32,256,128]{3,1,0,2:T(8,128)(2,1)S(1)} all-to-all(bf16[3,32,256,128]{3,1,0,2:T(8,128)(2,1)S(1)} %pad_maximum_fusion), channel_id=1, replica_groups=mesh['fs'=8,'tp'=4] {'tp'}, dimensions={2} | all-to-all | bytes 12582912 | tf_op jit(solution)/shard_map/all_to_all | solution.py:57
  98.0 7.6 %copy.89 = bf16[3,32,4,64,128]{4,2,3,1,0:T(4,128)(2,1)} copy(bf16[3,32,4,64,128]{4,1,0,3,2:T(8,128)(2,1)S(1)} %bitcast.37) | data formatting | bytes 12582912 | tf_op jit(solution)/shard_map/all_to_all | solution.py:57
  105.6 10.1 %all_to_all.29 = bf16[3,32,64,512]{3,2,1,0:T(8,128)(2,1)} reshape(bf16[3,32,64,4,128]{4,3,2,1,0:T(4,128)(2,1)} %bitcast.38) | data formatting | bytes 12582912 | tf_op jit(solution)/shard_map/all_to_all | solution.py:57
  115.7 22.5 %copy.71 = bf16[3,64,32,512]{1,0,3,2:T(4,128)(2,1)} copy(bf16[3,64,32,512]{3,1,2,0:T(8,128)(2,1)} %bitcast.40) | data formatting | bytes 12582912 | tf_op jit(solution)/shard_map/reshape | solution.py:13
  138.3 15.3 %reshape.55 = bf16[8,2,196608]{2,1,0:T(2,128)(2,1)} reshape(bf16[16384,3,64]{2,1,0:T(4,128)(2,1)} %bitcast.34) | data formatting | bytes 12582912
  153.6 144.3 %all_to_all.37 = bf16[8,2,196608]{2,1,0:T(2,128)(2,1)} all-to-all(bf16[8,2,196608]{2,1,0:T(2,128)(2,1)} %reshape.55), channel_id=1, replica_groups=mesh['fs'=8,'tp'=4] {'fs'}, dimensions={0} | all-to-all | bytes 12582912 | tf_op jit(solution)/shard_map/all_to_all | solution.py:58
  297.8 14.2 %reshape.56 = bf16[16384,3,64]{2,1,0:T(4,128)(2,1)} reshape(bf16[8,2,196608]{2,1,0:T(2,128)(2,1)} %all_to_all.37) | data formatting | bytes 12582912
  312.0 23.2 %copy.73 = bf16[3,64,8,2048]{3,1,2,0:T(8,128)(2,1)} copy(bf16[3,64,8,2048]{1,0,3,2:T(4,128)(2,1)} %bitcast.35) | data formatting | bytes 12582912 | tf_op jit(solution)/shard_map/all_to_all | solution.py:58
  335.3 0.0 copy-start.5
  335.3 0.0 copy-start.3
  335.3 0.0 copy-start.2
  335.3 0.0 copy-start.1
  335.3 0.0 all-gather.2.cloned.1.call-update
  335.3 0.3 reduce-scatter.2.cloned.1.call-start
  335.6 0.3 copy-done.5
  336.0 0.0 copy-done.3
  336.0 0.0 copy-done.2
  336.0 0.5 copy-done.1
  336.5 0.3 fusion.4
  336.8 223.6 %all-gather.2.cloned.1.call-done = bf16[3,2048,2048]{2,1,0:T(8,128)(2,1)} async-done(((bf16[3,512,2048]{2,1,0:T(8,128)(2,1)}), bf16[3,2048,2048]{2,1,0:T(8,128)(2,1)}) %all-gather.2.cloned.1.call-update) | async-done | bytes 25165840 | tf_op jit(solution)/shard_map/all_gather | solution.py:59
  560.4 16.8 %fusion.20 = (bf16[1,8,4,64,2048]{4,3,1,2,0:T(8,128)(2,1)}, bf16[1,8,4,64,2048]{4,3,1,2,0:T(8,128)(2,1)}, bf16[1,8,4,64,2048]{4,3,1,2,0:T(8,128)(2,1)}) fusion(bf16[3,8,4,64,2048]{4,3,1,2,0:T(8,128)(2,1)} %bitcast.36), kind=kLoop, calls=%fused_computation.39 | loop fusion | bytes 50331648 | tf_op jit(solution)/shard_map/slice | solution.py:60
  577.2 8.4 %copy.67 = bf16[1,8,4,64,2048]{4,3,2,1,0:T(8,128)(2,1)} copy(bf16[1,8,4,64,2048]{4,3,1,2,0:T(8,128)(2,1)} %get-tuple-element.30) | data formatting | bytes 16777216 | tf_op jit(solution)/shard_map/slice | solution.py:60
  585.7 8.4 %copy.68 = bf16[1,8,4,64,2048]{4,3,2,1,0:T(8,128)(2,1)} copy(bf16[1,8,4,64,2048]{4,3,1,2,0:T(8,128)(2,1)} %get-tuple-element.29) | data formatting | bytes 16777216 | tf_op jit(solution)/shard_map/slice | solution.py:60
  594.1 8.4 %copy.69 = bf16[1,8,4,64,2048]{4,3,2,1,0:T(8,128)(2,1)} copy(bf16[1,8,4,64,2048]{4,3,1,2,0:T(8,128)(2,1)} %get-tuple-element.28) | data formatting | bytes 16777216 | tf_op jit(solution)/shard_map/slice | solution.py:60
  602.5 5.8 convolution_multiply_fusion.1
  608.3 1.4 convolution_multiply_fusion.2
  609.7 11.8 %fusion.14 = f32[2048,256]{1,0:T(8,128)} fusion(bf16[2048,2048]{1,0:T(8,128)(2,1)} %bitcast.45, f32[256,2048]{1,0:T(8,128)S(1)} %convolution_multiply_fusion.2, bf16[2048,2048]{1,0:T(8,128)(2,1)} %bitcast.43, bf16[256,2048]{1,0:T(8,128)(2,1)S(1)} %copy-done.1, f32[256]{0:T(256)S(1)} %add_rsqrt_fusion), kind=kOutput, calls=%fused_computation.23 | convolution fusion | flops 4298113024 | bytes 22021120 | tf_op jit(solution)/shard_map/dot_general | solution.py:64
  621.5 0.0 reduce-scatter.2.cloned.1.call-update
  621.5 36.2 %reduce-scatter.2.cloned.1.call-done = f32[256,256]{1,0:T(8,128)} async-done(((f32[2048,256]{1,0:T(8,128)}), f32[256,256]{1,0:T(8,128)}) %reduce-scatter.2.cloned.1.call-update) | async-done | bytes 262160 | tf_op jit(solution)/shard_map/reduce_scatter | solution.py:63
  657.7 1.0 fusion.11
  658.7 0.8 copy.70
  (5 shorter events, 0.0 us)
Async XLA Ops:
  7.2 4.8 copy-start.4
  7.2 553.3 %all-gather.2.cloned.1.call-start = ((), (), s32[]{:S(2)}) async-start(), calls=%async_computation.3 | async-start | bytes 31457280 | tf_op jit(solution)/shard_map/all_gather | solution.py:59
  7.2 4.8 copy-start
  335.3 0.7 copy-start.5
  335.3 0.7 copy-start.3
  335.3 0.7 copy-start.2
  335.3 1.3 copy-start.1
  335.3 322.4 %reduce-scatter.2.cloned.1.call-start = ((), (), s32[]{:S(2)}) async-start(), calls=%async_computation.4 | async-start | bytes 2359296 | tf_op jit(solution)/shard_map/reduce_scatter | solution.py:63
Sparse Core Ops, SparseCore 0:
  335.4 224.9 all-gather.1
  621.7 35.9 reduce-scatter.1
where the time goes:
time: 669 us; the launch traced here: 666 us
  waiting for transfers between devices  260 us (39%)
  blocking collectives  220 us (33%)
  local copies, waits for them, and re-layouts  142 us (21%)
  matrix products  19 us (3%)
  between operations  14.1 us (2%)
  other arithmetic  12 us (2%)
    all_gather x1, waiting for transfers between devices, shards(): served = restore_rows(lax.all_gather(moved, 'tp', axis=1, tiled=True), rows)  224 us
    all_to_all x1, blocking collectives, shards(): lax.all_to_all(flatten_rows(widened), 'fs', split_axis=2, concat_axis=1,...  144 us
    all_to_all x1, blocking collectives, shards(): lax.all_to_all(stacked, 'tp', split_axis=2, concat_axis=3, tiled=True)  75.3 us
    slice x4, local copies, waits for them, and re-layouts, shards(): gate_local, up_local, down_local = (served[0], served[1], served[2])  42.1 us
    reduce_scatter x1, waiting for transfers between devices, shards(): lax.psum_scatter(lax.dot_general(down_local, scaled, (((1,), (1,)), ((),...  36.2 us
    unnamed x16, local copies, waits for them, and re-layouts  36 us
    all_to_all x1, local copies, waits for them, and re-layouts, shards(): lax.all_to_all(flatten_rows(widened), 'fs', split_axis=2, concat_axis=1,...  23.2 us
    reshape x1, local copies, waits for them, and re-layouts, flatten_rows(): return piece.transpose(0, 2, 1, 3).reshape(count, rows, experts * hidden)  22.5 us
  transfers between devices with their start and end apart: 2, of which 2 were waited for; matrix products, arithmetic and copies ran while one was open for 0% of the time, Pallas kernels for 0%

commit v1 on v0

--- a/solution.py
+++ b/solution.py
@@ -55,7 +55,10 @@
     weight = jnp.sum(member * route_weight[:, :, None], axis=1)
     stacked = jnp.stack([gate_cast, up_cast, down_cast])
     widened = lax.all_to_all(stacked, "tp", split_axis=2, concat_axis=3, tiled=True)
-    moved = lax.all_to_all(flatten_rows(widened), "fs", split_axis=2, concat_axis=1, tiled=True)
+    own = flatten_rows(widened)
+    pieces = jnp.split(own, lax.axis_size("fs"), axis=2)
+    got = lax.all_to_all(jnp.stack(pieces), "fs", 0, 0)
+    moved = jnp.concatenate(got, axis=1)
     served = restore_rows(lax.all_gather(moved, "tp", axis=1, tiled=True), rows)
     gate_local, up_local, down_local = (served[0], served[1], served[2])
     column_weight = route_columns(weight, gate_local.shape[1], experts)

time: 669 us -> 598 us (0.89)
  local copies, waits for them, and re-layouts: 142 us -> 73.5 us
    unnamed x16 -> x21, local copies, waits for them, and re-layouts: 36 us -> 6.84 us
    all_to_all x1 -> x0, local copies, waits for them, and re-layouts: 23.2 us -> none  [shards(): lax.all_to_all(flatten_rows(widened), 'fs', split_axis=2, concat_axis=1,...]
    reshape x1, local copies, waits for them, and re-layouts: 22.5 us -> 3.6 us  [flatten_rows(): return piece.transpose(0, 2, 1, 3).reshape(count, rows, experts * hidden)]
where the time goes in v1:
time: 598 us
  waiting for transfers between devices  260 us (43%)
  blocking collectives  219 us (37%)
  local copies, waits for them, and re-layouts  73.5 us (12%)
  matrix products  19 us (3%)
  between operations  14.2 us (2%)
  other arithmetic  12 us (2%)
    all_gather x1, waiting for transfers between devices, shards(): served = restore_rows(lax.all_gather(moved, 'tp', axis=1, tiled=True), rows)  224 us
    all_to_all x1, blocking collectives, shards(): got = lax.all_to_all(jnp.stack(pieces), 'fs', 0, 0)  144 us
    all_to_all x1, blocking collectives, shards(): lax.all_to_all(stacked, 'tp', split_axis=2, concat_axis=3, tiled=True)  75.3 us
    slice x4, local copies, waits for them, and re-layouts, shards(): gate_local, up_local, down_local = (served[0], served[1], served[2])  42.1 us
    reduce_scatter x1, waiting for transfers between devices, shards(): lax.psum_scatter(lax.dot_general(down_local, scaled, (((1,), (1,)), ((),...  36.1 us
    all_to_all x2, local copies, waits for them, and re-layouts, shards(): lax.all_to_all(stacked, 'tp', split_axis=2, concat_axis=3, tiled=True)  17.7 us
  transfers between devices with their start and end apart: 2, of which 2 were waited for; matrix products, arithmetic and copies ran while one was open for 0% of the time, Pallas kernels for 0%

profile of v1, /device:TPU:0, one launch (start us, length us, event | category | flops | bytes accessed | tf_op | source)
XLA Modules:
  0.0 597.6 jit_solution(17658314490734537751)
XLA Ops:
  7.2 0.0 copy-start.4
  7.2 0.0 all-gather.2.cloned.1.call-start
  7.2 0.0 copy-start
  7.2 4.8 copy.70
  12.0 0.0 copy-done.4
  12.0 0.0 copy-done
  12.0 9.9 %fusion.6 = (bf16[1,32,256,128]{3,1,0,2:T(8,128)(2,1)S(1)}, bf16[1,32,256,128]{3,1,0,2:T(8,128)(2,1)S(1)}) fusion(f32[32,256,128]{2,1,0:T(8,128)S(1)} %copy-done, f32[256]{0:T(256)S(1)} %copy-done.4, f32[32,256,128]{2,1,0:T(8,128)} %param.11), kind=kLoop, calls=%fused_computation.16 | loop fusion | flops 4194304 | bytes 12583936 | tf_op jit(solution)/shard_map/stack | solution.py:56
  22.0 0.8 pad_maximum_fusion
  22.7 75.3 %all_to_all.23 = bf16[3,32,256,128]{3,1,0,2:T(8,128)(2,1)S(1)} all-to-all(bf16[3,32,256,128]{3,1,0,2:T(8,128)(2,1)S(1)} %pad_maximum_fusion), channel_id=1, replica_groups=mesh['fs'=8,'tp'=4] {'tp'}, dimensions={2} | all-to-all | bytes 12582912 | tf_op jit(solution)/shard_map/all_to_all | solution.py:57
  98.0 7.6 %copy.69 = bf16[3,32,4,64,128]{4,2,3,1,0:T(4,128)(2,1)} copy(bf16[3,32,4,64,128]{4,1,0,3,2:T(8,128)(2,1)S(1)} %bitcast.72) | data formatting | bytes 12582912 | tf_op jit(solution)/shard_map/all_to_all | solution.py:57
  105.6 10.1 %all_to_all.19 = bf16[3,32,64,512]{3,2,1,0:T(8,128)(2,1)} reshape(bf16[3,32,64,4,128]{4,3,2,1,0:T(4,128)(2,1)} %bitcast.73) | data formatting | bytes 12582912 | tf_op jit(solution)/shard_map/all_to_all | solution.py:57
  115.7 3.6 copy.54
  119.3 0.1 fusion.16
  119.4 0.1 fusion.15
  119.4 0.1 fusion.14
  119.5 0.1 fusion.13
  119.6 0.1 fusion.12
  119.6 0.1 fusion.11
  119.7 0.1 fusion.10
  119.7 0.1 fusion.9
  119.8 143.6 %all_to_all.24 = bf16[8,3,64,2048]{3,2,1,0:T(8,128)(2,1)S(1)} all-to-all(bf16[8,3,64,2048]{3,2,1,0:T(8,128)(2,1)S(1)} %fusion.9), channel_id=1, replica_groups=mesh['fs'=8,'tp'=4] {'fs'}, dimensions={0} | all-to-all | bytes 12582912 | tf_op jit(solution)/shard_map/all_to_all | solution.py:60
  263.4 3.3 copy.49
  266.7 0.0 copy-start.5
  266.7 0.0 copy-start.3
  266.7 0.0 copy-start.2
  266.7 0.0 copy-start.1
  266.7 0.0 all-gather.2.cloned.1.call-update
  266.7 0.3 reduce-scatter.2.cloned.1.call-start
  267.0 0.3 copy-done.5
  267.4 0.0 copy-done.3
  267.4 0.0 copy-done.2
  267.4 0.5 copy-done.1
  268.0 0.3 fusion.4
  268.2 223.6 %all-gather.2.cloned.1.call-done = bf16[3,2048,2048]{2,1,0:T(8,128)(2,1)} async-done(((bf16[3,512,2048]{2,1,0:T(8,128)(2,1)}), bf16[3,2048,2048]{2,1,0:T(8,128)(2,1)}) %all-gather.2.cloned.1.call-update) | async-done | bytes 25165840 | tf_op jit(solution)/shard_map/all_gather | solution.py:62
  491.9 16.8 %fusion.28 = (bf16[1,8,4,64,2048]{4,3,1,2,0:T(8,128)(2,1)}, bf16[1,8,4,64,2048]{4,3,1,2,0:T(8,128)(2,1)}, bf16[1,8,4,64,2048]{4,3,1,2,0:T(8,128)(2,1)}) fusion(bf16[3,8,4,64,2048]{4,3,1,2,0:T(8,128)(2,1)} %bitcast.62), kind=kLoop, calls=%fused_computation.55 | loop fusion | bytes 50331648 | tf_op jit(solution)/shard_map/slice | solution.py:63
  508.6 8.4 %copy.50 = bf16[1,8,4,64,2048]{4,3,2,1,0:T(8,128)(2,1)} copy(bf16[1,8,4,64,2048]{4,3,1,2,0:T(8,128)(2,1)} %get-tuple-element.26) | data formatting | bytes 16777216 | tf_op jit(solution)/shard_map/slice | solution.py:63
  517.1 8.4 %copy.51 = bf16[1,8,4,64,2048]{4,3,2,1,0:T(8,128)(2,1)} copy(bf16[1,8,4,64,2048]{4,3,1,2,0:T(8,128)(2,1)} %get-tuple-element.25) | data formatting | bytes 16777216 | tf_op jit(solution)/shard_map/slice | solution.py:63
  525.5 8.4 %copy.52 = bf16[1,8,4,64,2048]{4,3,2,1,0:T(8,128)(2,1)} copy(bf16[1,8,4,64,2048]{4,3,1,2,0:T(8,128)(2,1)} %get-tuple-element.24) | data formatting | bytes 16777216 | tf_op jit(solution)/shard_map/slice | solution.py:63
  534.0 5.8 convolution_multiply_fusion.1
  539.7 1.4 convolution_multiply_fusion.2
  541.1 11.8 %fusion.22 = f32[2048,256]{1,0:T(8,128)} fusion(bf16[2048,2048]{1,0:T(8,128)(2,1)} %bitcast.80, f32[256,2048]{1,0:T(8,128)S(1)} %convolution_multiply_fusion.2, bf16[2048,2048]{1,0:T(8,128)(2,1)} %bitcast.78, bf16[256,2048]{1,0:T(8,128)(2,1)S(1)} %copy-done.1, f32[256]{0:T(256)S(1)} %add_rsqrt_fusion), kind=kOutput, calls=%fused_computation.39 | convolution fusion | flops 4298113024 | bytes 22021120 | tf_op jit(solution)/shard_map/dot_general | solution.py:67
  552.9 0.0 reduce-scatter.2.cloned.1.call-update
  553.0 36.1 %reduce-scatter.2.cloned.1.call-done = f32[256,256]{1,0:T(8,128)} async-done(((f32[2048,256]{1,0:T(8,128)}), f32[256,256]{1,0:T(8,128)}) %reduce-scatter.2.cloned.1.call-update) | async-done | bytes 262160 | tf_op jit(solution)/shard_map/reduce_scatter | solution.py:66
  589.1 1.0 fusion.19
  590.0 0.8 copy.53
  (5 shorter events, 0.0 us)
Async XLA Ops:
  7.2 4.8 copy-start.4
  7.2 484.7 %all-gather.2.cloned.1.call-start = ((), (), s32[]{:S(2)}) async-start(), calls=%async_computation.3 | async-start | bytes 31457280 | tf_op jit(solution)/shard_map/all_gather | solution.py:62
  7.2 4.8 copy-start
  266.7 0.7 copy-start.5
  266.7 0.7 copy-start.3
  266.7 0.7 copy-start.2
  266.7 1.3 copy-start.1
  266.7 322.3 %reduce-scatter.2.cloned.1.call-start = ((), (), s32[]{:S(2)}) async-start(), calls=%async_computation.4 | async-start | bytes 2359296 | tf_op jit(solution)/shard_map/reduce_scatter | solution.py:66
Sparse Core Ops, SparseCore 0:
  266.8 224.9 all-gather.1
  553.1 35.9 reduce-scatter.1
